TPU v7x, 128 devices: a whole 4x4x4 slice. The times are simulated.
128 devices in a mesh: sp: 32 (over z, y, core), tp: 4 (over x).
Axes of the slice: x: 4, y: 4, z: 4, core: 2. Of those that a mesh axis runs over, the one named last changes fastest.
Arguments:
- tokens: bfloat16 [32768, 2048], P('sp', 'tp'), may hold values from -6 to 6
- input_norm_gain: float32 [2048], replicated, may hold values from 0.1 to 1.9
- pooling_input_matrix: bfloat16 [2048, 512], P(None, 'tp'), may hold values from -0.125 to 0.125
- query_projection_matrix: bfloat16 [2048, 1024], P(None, 'tp'), may hold values from -0.125 to 0.125
- key_projection_matrix: bfloat16 [2048, 1024], P(None, 'tp'), may hold values from -0.125 to 0.125
- value_projection_matrix: bfloat16 [2048, 1024], P(None, 'tp'), may hold values from -0.125 to 0.125
- output_gate_matrix: bfloat16 [2048, 1024], P(None, 'tp'), may hold values from -0.125 to 0.125
- input_gate_matrix: bfloat16 [2048, 2, 8], replicated
- forget_gate_matrix: bfloat16 [2048, 2, 8], replicated, may hold values from -0.125 to 0.125
- forget_gate_bias: float32 [2, 8], replicated
- log_forget_scale: float32 [2, 32768], P(None, 'sp'), may hold values from 0.35 to 2.8
- extra_log_forget: float32 [2, 32768], P(None, 'sp'), may hold values from -0.7 to 0, as said below
- starting_memory: float32 [2, 8, 128, 128], P(None, 'tp'), may hold values from -3 to 3
- starting_normalizer: float32 [2, 8, 128], P(None, 'tp'), may hold values from -3 to 3
- starting_log_scale: float32 [2, 8], P(None, 'tp'), may hold values from 2 to 5
- pooling_group_map: bfloat16 [4, 128, 128], replicated, may hold values from -0.5 to 0.5
- pooling_channel_scale: float32 [512], replicated, may hold values from 0.1 to 1.9
- memory_head_gain: float32 [1024], replicated, may hold values from 0.1 to 1.9
- pooling_output_matrix: bfloat16 [512, 2048], replicated, may hold values from -0.25 to 0.25
- memory_output_matrix: bfloat16 [1024, 2048], replicated, may hold values from -0.1875 to 0.1875
Outputs:
- mixed_out: bfloat16 [32768, 2048], P(('sp', 'tp'))
Inputs may be any that keep to these rules, and one draw needn't show every extreme that they name: `extra_log_forget`: at most three nonzero entries in each direction.
All inputs are finite; a program needn't handle non-finite values.
Results may differ from a plain program's by a relative error of at most 0.0091.
Values may be sent and summed in bfloat16 or wider, within the bound.
A program may use at most 128 MiB of HBM per device.

v0:
```python
import jax
import jax.numpy as jnp
from jax import lax
from jax.sharding import PartitionSpec as P

DH = 128
BLOCK = 128
NEG_BIG = -1e30
LN_EPS = 1e-05
HEAD_EPS = 1e-06
RIM_ROWS = 8


def extended(block, sides, width):
    for axis, dim in sides:
        count = lax.axis_size(axis)
        forward = [(i, i + 1) for i in range(count - 1)]
        backward = [(target, source) for source, target in forward]
        low = lax.ppermute(
            lax.slice_in_dim(block, block.shape[dim] - width, None, axis=dim), axis, forward
        )
        high = lax.ppermute(lax.slice_in_dim(block, 0, width, axis=dim), axis, backward)
        block = jnp.concatenate([low, block, high], axis=dim)
    return block


def block_step(carried, pieces):
    memory, normer, maxlog = carried
    q_blk, k_blk, v_blk, i_blk, f_blk = pieces
    lower_mask = jnp.tril(jnp.ones((BLOCK, BLOCK), dtype=bool))
    cumulative = jnp.cumsum(f_blk, axis=-1)
    exponent = jnp.where(
        lower_mask, cumulative[:, :, None] - cumulative[:, None, :] + i_blk[:, None, :], NEG_BIG
    )
    carried_log = cumulative + maxlog[:, None]
    row_max = jnp.maximum(carried_log, exponent.max(-1))
    fading = jnp.exp(carried_log - row_max)
    scores = jnp.einsum("htd,hsd->hts", q_blk, k_blk) * jnp.exp(exponent - row_max[:, :, None])
    numerator = fading[:, :, None] * jnp.einsum("hvk,htk->htv", memory, q_blk) + jnp.einsum(
        "hts,hsv->htv", scores, v_blk
    )
    denominator = fading * jnp.einsum("hk,htk->ht", normer, q_blk) + scores.sum(-1)
    summed = cumulative[:, -1]
    weight_log = summed[:, None] - cumulative + i_blk
    new_max = jnp.maximum(summed + maxlog, weight_log.max(-1))
    carry_scale = jnp.exp(summed + maxlog - new_max)
    weights = jnp.exp(weight_log - new_max[:, None])
    memory = carry_scale[:, None, None] * memory + jnp.einsum(
        "hsv,hsk->hvk", v_blk * weights[:, :, None], k_blk
    )
    normer = carry_scale[:, None] * normer + jnp.einsum("hs,hsk->hk", weights, k_blk)
    return ((memory, normer, new_max), (numerator, denominator, row_max))


def to_blocks(source):
    return jnp.moveaxis(
        source.reshape((source.shape[0], source.shape[1] // BLOCK, BLOCK) + source.shape[2:]), 1, 0
    )


def from_blocks(source):
    return jnp.moveaxis(source, 0, 1).reshape(
        (source.shape[1], source.shape[0] * source.shape[2]) + source.shape[3:]
    )


def local_pass(query_heads, key_heads, value_heads, log_in, log_forget_gate):
    head_count = query_heads.shape[0]
    head_size = query_heads.shape[2]
    initial = (
        jnp.zeros((head_count, head_size, head_size), jnp.float32),
        jnp.zeros((head_count, head_size), jnp.float32),
        jnp.full((head_count,), NEG_BIG, jnp.float32),
    )
    finals, outputs = lax.scan(
        block_step,
        initial,
        tuple(
            (
                to_blocks(member)
                for member in (query_heads, key_heads, value_heads, log_in, log_forget_gate)
            )
        ),
    )
    numerator, denominator, row_max = (from_blocks(member) for member in outputs)
    falls = jnp.cumsum(log_forget_gate, axis=1)
    return ((falls[:, -1],) + finals, (numerator, denominator, row_max, falls))


def join_states(earlier, later):
    early_fall, early_memory, early_normer, early_max = earlier
    late_fall, late_memory, late_normer, late_max = later
    merged_max = jnp.maximum(early_max + late_fall, late_max)
    early_weight = jnp.exp(early_max + late_fall - merged_max)
    late_weight = jnp.exp(late_max - merged_max)
    return (
        late_fall,
        early_weight[..., None, None] * early_memory + late_weight[..., None, None] * late_memory,
        early_weight[..., None] * early_normer + late_weight[..., None] * late_normer,
        merged_max,
    )


def prefix_from_all(gathered, position, from_later):
    falls, memories, normers, maxima = gathered
    order = jnp.arange(falls.shape[0], dtype=jnp.int32)
    inclusive = jnp.cumsum(falls, axis=0)
    exclusive = inclusive - falls
    if from_later:
        valid = order > position
        between = exclusive - inclusive[position][None]
        total_fall = inclusive[-1] - inclusive[position]
    else:
        valid = order < position
        between = exclusive[position][None] - inclusive
        total_fall = exclusive[position]
    log_weight = jnp.where(valid[:, None], maxima + between, NEG_BIG)
    joint_max = jnp.max(log_weight, axis=0)
    weights = jnp.where(valid[:, None], jnp.exp(log_weight - joint_max[None]), 0.0)
    memory = jnp.einsum("jh,jhvk->hvk", weights, memories)
    normer = jnp.einsum("jh,jhk->hk", weights, normers)
    return (total_fall, memory, normer, joint_max)


def finish(local_terms, entering, query_heads):
    numerator, denominator, row_max, falls = local_terms
    fall_in, memory, normer, max_in = entering
    state_log = falls + max_in[:, None]
    joint_max = jnp.maximum(row_max, state_log)
    local_weight = jnp.exp(row_max - joint_max)
    state_weight = jnp.exp(state_log - joint_max)
    full_numerator = local_weight[..., None] * numerator + state_weight[..., None] * jnp.einsum(
        "hvk,htk->htv", memory, query_heads
    )
    full_denominator = local_weight * denominator + state_weight * jnp.einsum(
        "hk,htk->ht", normer, query_heads
    )
    return full_numerator / jnp.maximum(jnp.abs(full_denominator), 1.0)[..., None]


def per_device(
    tokens,
    input_norm_gain,
    pooling_input_matrix,
    query_projection_matrix,
    key_projection_matrix,
    value_projection_matrix,
    output_gate_matrix,
    input_gate_matrix,
    forget_gate_matrix,
    forget_gate_bias,
    log_forget_scale,
    extra_log_forget,
    starting_memory,
    starting_normalizer,
    starting_log_scale,
    pooling_group_map,
    pooling_channel_scale,
    memory_head_gain,
    pooling_output_matrix,
    memory_output_matrix,
):
    local_rows = tokens.shape[0]
    own_width = tokens.shape[1]
    model_width = own_width * lax.axis_size("tp")
    group_index = lax.axis_index("tp")
    seq_index = lax.axis_index("sp")
    group_dim = pooling_input_matrix.shape[1]
    head_local = query_projection_matrix.shape[1] // DH
    mem_width = head_local * DH
    main_weight = jnp.concatenate(
        [
            pooling_input_matrix,
            query_projection_matrix,
            key_projection_matrix,
            value_projection_matrix,
            output_gate_matrix,
        ],
        axis=1,
    )
    gate_in = lax.dynamic_slice_in_dim(input_gate_matrix, group_index * head_local, head_local, 2)
    gate_fg = lax.dynamic_slice_in_dim(forget_gate_matrix, group_index * head_local, head_local, 2)
    gate_weight = jnp.concatenate([gate_in, gate_fg], axis=1).reshape(model_width, 4 * head_local)
    whole_rows = lax.all_gather(tokens, "tp", axis=1, tiled=True)
    floats = whole_rows.astype(jnp.float32)
    mean_row = jnp.sum(floats, axis=1) / model_width
    variance = jnp.sum(floats * floats, axis=1) / model_width - mean_row * mean_row
    normed = (
        (floats - mean_row[:, None]) * lax.rsqrt(variance + LN_EPS)[:, None] * input_norm_gain
    ).astype(jnp.bfloat16)
    projected = jnp.dot(normed, main_weight, preferred_element_type=jnp.float32)
    gate_pre = jnp.dot(normed, gate_weight, preferred_element_type=jnp.float32)
    pool_in = projected[:, :group_dim].astype(jnp.bfloat16)
    queries = projected[:, group_dim : group_dim + mem_width].astype(jnp.bfloat16)
    key_rows = projected[:, group_dim + mem_width : group_dim + 2 * mem_width].astype(jnp.bfloat16)
    value_rows = projected[:, group_dim + 2 * mem_width : group_dim + 3 * mem_width].astype(
        jnp.bfloat16
    )
    out_gate = projected[:, group_dim + 3 * mem_width :].astype(jnp.bfloat16)
    gate_pre = gate_pre.reshape(local_rows, 2, 2, head_local)
    log_in = gate_pre[:, 0]
    bias_own = lax.dynamic_slice_in_dim(forget_gate_bias, group_index * head_local, head_local, 1)
    log_forget_gate = (
        jax.nn.log_sigmoid(gate_pre[:, 1] + bias_own[None]) * log_forget_scale.T[:, :, None]
        + extra_log_forget.T[:, :, None]
    )

    def heads_of(source, factor):
        return (
            (source.astype(jnp.float32) * factor)
            .reshape(local_rows, head_local, DH)
            .transpose(1, 0, 2)
        )

    query_heads = heads_of(queries, 1.0)
    key_heads = heads_of(key_rows, DH ** (-0.5))
    value_heads = heads_of(value_rows, 1.0)
    forward_summary, forward_local = local_pass(
        query_heads, key_heads, value_heads, log_in[:, 0].T, log_forget_gate[:, 0].T
    )
    flipped_query = query_heads[:, ::-1]
    backward_summary, backward_local = local_pass(
        flipped_query,
        key_heads[:, ::-1],
        value_heads[:, ::-1],
        log_in[:, 1].T[:, ::-1],
        log_forget_gate[:, 1].T[:, ::-1],
    )
    rimmed = extended(pool_in, (("sp", 0),), RIM_ROWS).astype(jnp.float32)
    half_span = jnp.left_shift(jnp.int32(1), group_index)
    grouped = pool_in.astype(jnp.float32)
    pooled = jnp.zeros_like(grouped)
    for offset in range(-RIM_ROWS, RIM_ROWS):
        inside = ((offset >= -half_span) & (offset < half_span)).astype(jnp.float32)
        pooled = pooled + inside * rimmed[RIM_ROWS + offset : RIM_ROWS + offset + local_rows]
    positions = seq_index * local_rows + jnp.arange(local_rows, dtype=jnp.int32)
    total_rows = local_rows * lax.axis_size("sp")
    counts = (
        jnp.minimum(positions + half_span, total_rows) - jnp.maximum(positions - half_span, 0)
    ).astype(jnp.float32)
    contrast = (pooled / counts[:, None] - grouped).astype(jnp.bfloat16)
    map_own = lax.dynamic_index_in_dim(pooling_group_map, group_index, 0, keepdims=False)
    scale_own = lax.dynamic_slice_in_dim(
        pooling_channel_scale, group_index * group_dim, group_dim, 0
    )
    pool_out = (jnp.dot(contrast, map_own, preferred_element_type=jnp.float32) * scale_own).astype(
        jnp.bfloat16
    )
    stacked = tuple(
        (
            jnp.stack([forward_part, backward_part])[None]
            for forward_part, backward_part in zip(forward_summary, backward_summary)
        )
    )
    gathered = lax.all_gather(stacked, "sp", axis=0, tiled=True)
    forward_prefix = prefix_from_all(tuple((member[:, 0] for member in gathered)), seq_index, False)
    backward_prefix = prefix_from_all(tuple((member[:, 1] for member in gathered)), seq_index, True)

    def initial_state(direction):
        return (
            jnp.zeros((head_local,), jnp.float32),
            starting_memory[direction],
            starting_normalizer[direction],
            starting_log_scale[direction],
        )

    forward = finish(forward_local, join_states(initial_state(0), forward_prefix), query_heads)
    backward = finish(backward_local, join_states(initial_state(1), backward_prefix), flipped_query)
    hidden = forward + backward[:, ::-1]
    head_mean = jnp.mean(hidden, axis=-1, keepdims=True)
    head_var = jnp.mean(jnp.square(hidden - head_mean), axis=-1, keepdims=True)
    gain_heads = lax.dynamic_slice_in_dim(
        memory_head_gain, group_index * mem_width, mem_width, 0
    ).reshape(head_local, DH)
    scaled = (hidden - head_mean) * lax.rsqrt(head_var + HEAD_EPS) * gain_heads[:, None, :]
    mem_out = (
        scaled.transpose(1, 0, 2).reshape(local_rows, mem_width)
        * jax.nn.sigmoid(out_gate.astype(jnp.float32))
    ).astype(jnp.bfloat16)
    mixed = jnp.concatenate([pool_out, mem_out], axis=1)
    owned = lax.all_to_all(mixed, "tp", split_axis=0, concat_axis=1, tiled=True)
    owner_rows = owned.shape[0]
    owned = owned.reshape(owner_rows, lax.axis_size("tp"), group_dim + mem_width)
    pool_part = owned[:, :, :group_dim].reshape(owner_rows, lax.axis_size("tp") * group_dim)
    mem_part = owned[:, :, group_dim:].reshape(owner_rows, lax.axis_size("tp") * mem_width)
    result = jnp.dot(
        pool_part, pooling_output_matrix, preferred_element_type=jnp.float32
    ) + jnp.dot(mem_part, memory_output_matrix, preferred_element_type=jnp.float32)
    return result.astype(jnp.bfloat16)


def solution(mesh):
    placed = (
        P("sp", "tp"),
        P(),
        P(None, "tp"),
        P(None, "tp"),
        P(None, "tp"),
        P(None, "tp"),
        P(None, "tp"),
        P(),
        P(),
        P(),
        P(None, "sp"),
        P(None, "sp"),
        P(None, "tp", None, None),
        P(None, "tp", None),
        P(None, "tp"),
        P(),
        P(),
        P(),
        P(),
        P(),
    )
    return jax.shard_map(
        per_device, mesh=mesh, in_specs=placed, out_specs=P(("sp", "tp"), None), check_vma=False
    )
```

profile of v0, /device:TPU:1, one launch (start us, length us, event | category | flops | bytes accessed | tf_op | source)
XLA Modules:
  0.0 383.7 jit_solution(3305362146877481871)
XLA Ops:
  11.3 2.3 constant_dynamic-update-slice_fusion.7
  16.9 43.3 %all-gather.9.cloned.1.call-done = bf16[1024,2048]{1,0:T(8,128)(2,1)} async-done(((bf16[1024,512]{1,0:T(8,128)(2,1)}), bf16[1024,2048]{1,0:T(8,128)(2,1)}) %all-gather.9.cloned.1.call-update) | async-done | bytes 4194320 | tf_op jit(solution)/shard_map/all_gather | solution.py:184
  60.2 3.6 convert_reduce_fusion
  63.9 8.5 %convolution_convert_fusion = bf16[1024,1152]{1,0:T(8,128)(2,1)S(1)} fusion(bf16[2048,1152]{1,0:T(8,128)(2,1)} %constant_dynamic-update-slice_fusion.4, bf16[1024,2048]{1,0:T(8,128)(2,1)S(1)} %copy-done.5, f32[2048]{0:T(1024)S(1)} %copy-done.21, f32[1024]{0:T(1024)S(1)} %get-tuple-element.398, f32[1024]{0:T(1024)S(1)} %get-tuple-element.397), kind=kOutput, calls=%fused_computation.125 | convolution fusion | flops 4843503616 | bytes 11288576 | tf_op jit(solution)/shard_map/dot_general | solution.py:191
  75.9 5.1 %rev.22 = bf16[2,1024,128]{2,1,0:T(8,128)(2,1)} reverse(bf16[2,1024,128]{2,1,0:T(8,128)(2,1)S(1)} %get-tuple-element.407), dimensions={1} | reverse | bytes 1048576 | tf_op jit(solution)/shard_map/rev | solution.py:221
  81.0 3.7 fusion.70
  87.6 5.1 %rev.20 = f32[2,1024,128]{2,1,0:T(8,128)} reverse(f32[2,1024,128]{2,1,0:T(8,128)S(1)} %bitcast.498), dimensions={1} | reverse | bytes 2097152 | tf_op jit(solution)/shard_map/rev | solution.py:225
  92.7 8.2 %rev.21 = bf16[2,1024,128]{2,1,0:T(8,128)(2,1)} reverse(bf16[2,1024,128]{2,1,0:T(8,128)(2,1)} %get-tuple-element.381), dimensions={1} | reverse | bytes 1048576 | tf_op jit(solution)/shard_map/rev | solution.py:224
  104.0 66.0 %while.43 = (s32[]{:T(128)}, f32[2,128,128]{2,1,0:T(8,128)S(1)}, f32[2,128]{1,0:T(2,128)S(1)}, f32[2]{0:T(128)S(1)}, f32[8,2,128,128]{3,2,1,0:T(8,128)}, /*index...) while((s32[]{:T(128)}, f32[2,128,128]{2,1,0:T(8,128)S(1)}, ...), condition=%wide.region_18.19_spmd.clone, body=%wide.region_13.18_spmd.clone.sunk | while | flops 34327816 | bytes 1600317 | solution.py:75
  172.9 58.1 %while.42 = (s32[]{:T(128)}, f32[2,128,128]{2,1,0:T(8,128)S(1)}, f32[2,128]{1,0:T(2,128)S(1)}, f32[2]{0:T(128)S(1)}, f32[8,2,128,128]{3,2,1,0:T(8,128)}, /*index...) while((s32[]{:T(128)}, f32[2,128,128]{2,1,0:T(8,128)S(1)}, ...), condition=%wide.region_7.8_spmd.clone, body=%wide.region_2.7_spmd.clone.sunk | while | flops 34327816 | bytes 1600821 | solution.py:75
  236.3 25.2 %all-gather.4 = f32[32,2,2]{2,1,0:T(2,128)S(1)} all-gather(f32[1,2,2]{2,1,0:T(2,128)S(1)} %maximum_bitcast_fusion), channel_id=2, replica_groups=mesh['sp'=32,'tp'=4] {'sp'}, dimensions={0}, use_global_device_ids=true | all-gather | bytes 528 | tf_op jit(solution)/shard_map/all_gather | solution.py:255
  261.7 23.6 %all-gather.5 = f32[32,2,2]{2,1,0:T(2,128)S(1)} all-gather(f32[1,2,2]{2,1,0:T(2,128)S(1)} %maximum_bitcast_fusion.1), channel_id=3, replica_groups=mesh['sp'=32,'tp'=4] {'sp'}, dimensions={0}, use_global_device_ids=true | all-gather | bytes 528 | tf_op jit(solution)/shard_map/all_gather | solution.py:255
  286.8 2.1 collective-permute-start.1
  288.9 3.5 collective-permute-start
  292.4 22.6 %all-gather.3 = bf16[64,2,128]{2,1,0:T(2,128)(2,1)S(1)} all-gather(bf16[2,2,128]{2,1,0:T(2,128)(2,1)S(1)} %pad_maximum_fusion.3), channel_id=5, replica_groups=mesh['sp'=32,'tp'=4] {'sp'}, dimensions={0}, use_global_device_ids=true | all-gather | bytes 33792 | tf_op jit(solution)/shard_map/all_gather | solution.py:255
  318.4 2.6 copy.115
  321.0 2.4 reshape.649
  324.9 2.4 reshape.646
  327.4 2.1 fusion.82
  329.5 4.2 %slice_bitcast_fusion.1 = (bf16[32,2,128,128]{3,2,1,0:T(8,128)(2,1)}, bf16[32,2,128,128]{3,2,1,0:T(8,128)(2,1)S(1)}) fusion(bf16[32,2,2,128,128]{4,3,2,1,0:T(8,128)(2,1)} %bitcast.502), kind=kLoop, calls=%fused_computation.118 | loop fusion | bytes 8388608 | tf_op jit(solution)/shard_map/squeeze | solution.py:256
  336.4 9.4 %rev.23 = f32[2,1024,128]{1,2,0:T(8,128)} reverse(f32[2,1024,128]{1,2,0:T(8,128)} %fusion.81), dimensions={1} | reverse | bytes 2097152 | tf_op jit(solution)/shard_map/rev | solution.py:269
  345.7 2.8 fusion.74
  356.0 15.5 %all_to_all.16 = bf16[4,256,384]{1,2,0:T(8,128)(2,1)S(1)} all-to-all(bf16[4,256,384]{1,2,0:T(8,128)(2,1)} %copy.118), channel_id=1, replica_groups=mesh['sp'=32,'tp'=4] {'tp'}, dimensions={0} | all-to-all | bytes 1572864 | tf_op jit(solution)/shard_map/all_to_all | solution.py:281
  371.6 3.5 fusion.178
  (446 shorter events, 167.2 us)
Async XLA Ops:
  6.5 368.6 %copy-start = (bf16[512,2048]{1,0:T(8,128)(2,1)S(1)}, bf16[512,2048]{1,0:T(8,128)(2,1)}, u32[]{:S(2)}) copy-start(bf16[512,2048]{1,0:T(8,128)(2,1)} %param.42) | copy-start | bytes 6291460
  6.5 7.1 %copy-start.8 = (bf16[2048,256]{1,0:T(8,128)(2,1)S(1)}, bf16[2048,256]{1,0:T(8,128)(2,1)}, u32[]{:S(2)}) copy-start(bf16[2048,256]{1,0:T(8,128)(2,1)} %param.28) | copy-start | bytes 3145732
  6.5 53.7 %all-gather.9.cloned.1.call-start = ((), (), s32[]{:S(2)}) async-start(), calls=%async_computation.1 | async-start | bytes 5242880 | tf_op jit(solution)/shard_map/all_gather | solution.py:184
  7.3 322.2 %all-gather.11.cloned.1.call-start = ((), (), s32[]{:S(2)}) async-start(), calls=%async_computation.2 | async-start | bytes 4325376 | tf_op jit(solution)/shard_map/all_gather | solution.py:255
  8.4 6.2 %copy-start.9 = (bf16[2048,256]{1,0:T(8,128)(2,1)S(1)}, bf16[2048,256]{1,0:T(8,128)(2,1)}, u32[]{:S(2)}) copy-start(bf16[2048,256]{1,0:T(8,128)(2,1)} %param.29) | copy-start | bytes 3145732
  8.5 7.3 %copy-start.10 = (bf16[2048,256]{1,0:T(8,128)(2,1)S(1)}, bf16[2048,256]{1,0:T(8,128)(2,1)}, u32[]{:S(2)}) copy-start(bf16[2048,256]{1,0:T(8,128)(2,1)} %param.30) | copy-start | bytes 3145732
  14.7 49.2 %copy-start.21 = (f32[2048]{0:T(1024)S(1)}, f32[2048]{0:T(1024)}, u32[]{:S(2)}) copy-start(f32[2048]{0:T(1024)} %param.25) | copy-start | bytes 24580
  60.2 3.6 copy-start.5
  75.9 8.8 %copy-start.3 = (bf16[2,1024,128]{2,1,0:T(8,128)(2,1)}, bf16[2,1024,128]{2,1,0:T(8,128)(2,1)S(1)}, u32[]{:S(2)}) copy-start(bf16[2,1024,128]{2,1,0:T(8,128)(2,1)S(1)} %get-tuple-element.407) | copy-start | bytes 1572868
  81.0 3.7 copy-start.12
  81.0 3.7 copy-start.13
  172.9 113.0 %copy-start.15 = (f32[2,2]{1,0:T(2,128)S(1)}, f32[2,2]{1,0:T(2,128)}, u32[]{:S(2)}) copy-start(f32[2,2]{1,0:T(2,128)} %param.38) | copy-start | bytes 52
  172.9 142.5 %copy-start.14 = (f32[2,2,128]{2,1,0:T(2,128)S(1)}, f32[2,2,128]{2,1,0:T(2,128)}, u32[]{:S(2)}) copy-start(f32[2,2,128]{2,1,0:T(2,128)} %param.37) | copy-start | bytes 6148
  231.0 92.6 %copy-start.6 = (f32[8,2,128,128]{3,2,1,0:T(8,128)S(1)}, f32[8,2,128,128]{3,2,1,0:T(8,128)}, u32[]{:S(2)}) copy-start(f32[8,2,128,128]{3,2,1,0:T(8,128)} %get-tuple-element.142) | copy-start | bytes 3145732
  286.8 40.5 %collective-permute-start.1 = (bf16[8,128]{1,0:T(8,128)(2,1)S(1)}, bf16[8,128]{1,0:T(8,128)(2,1)S(1)}, u32[]{:S(2)}, u32[]{:S(2)}) collective-permute-start(bf16[8,128]{1,0:T(8,128)(2,1)S(1)} %get-tuple-element.374), channel_id=1, source_target_pairs={{4,0},{8,4},{12,8},{16,12},{20,16},{24,20},{28,24},{32,28},{36,32}... | collective-permute-start | bytes 6152 | tf_op jit(solution)/shard_map/ppermute | solution.py:22
  288.9 38.4 %collective-permute-start = (bf16[8,128]{1,0:T(8,128)(2,1)S(1)}, bf16[8,128]{1,0:T(8,128)(2,1)S(1)}, u32[]{:S(2)}, u32[]{:S(2)}) collective-permute-start(bf16[8,128]{1,0:T(8,128)(2,1)S(1)} %get-tuple-element.373), channel_id=1, source_target_pairs={{0,4},{4,8},{8,12},{12,16},{16,20},{20,24},{24,28},{28,32},{32,36}... | collective-permute-start | bytes 6152 | tf_op jit(solution)/shard_map/ppermute | solution.py:19
  318.4 8.9 %slice-start = ((bf16[1024,1152]{1,0:T(8,128)(2,1)}), bf16[1024,128]{1,0:T(8,128)(2,1)S(1)}, s32[]{:S(2)}) async-start(bf16[1024,1152]{1,0:T(8,128)(2,1)} %copy-done.7), calls=%async_computation.3 | async-start | bytes 524288 | tf_op jit(solution)/shard_map/slice | solution.py:193
  318.4 8.9 %copy-start.22 = (f32[128]{0:T(128)S(1)}, f32[128]{0:T(128)}, u32[]{:S(2)}) copy-start(f32[128]{0:T(128)} %dynamic_slice.60) | copy-start | bytes 1540
  329.5 5.5 %copy-start.4 = (bf16[2,1024,128]{2,1,0:T(8,128)(2,1)S(1)}, bf16[2,1024,128]{2,1,0:T(8,128)(2,1)}, u32[]{:S(2)}) copy-start(bf16[2,1024,128]{2,1,0:T(8,128)(2,1)} %rev.22) | copy-start | bytes 1572868
  329.5 5.5 %copy-start.11 = (f32[2,1024,128]{1,2,0:T(8,128)S(1)}, f32[2,1024,128]{1,2,0:T(8,128)}, u32[]{:S(2)}) copy-start(f32[2,1024,128]{1,2,0:T(8,128)} %reshape.649) | copy-start | bytes 3145732
  329.5 5.5 %copy-start.19 = (f32[2]{0:T(128)S(1)}, f32[2]{0:T(128)}, u32[]{:S(2)}) copy-start(f32[2]{0:T(128)} %copy-done.18) | copy-start | bytes 28
  329.5 5.5 %copy-start.20 = (f32[2,2,128,128]{3,2,1,0:T(8,128)S(1)}, f32[2,2,128,128]{3,2,1,0:T(8,128)}, u32[]{:S(2)}) copy-start(f32[2,2,128,128]{3,2,1,0:T(8,128)} %param.36) | copy-start | bytes 786436
  335.0 13.6 %copy-start.2 = (bf16[128,2,8,128]{3,2,1,0:T(8,128)(2,1)S(1)}, bf16[128,2,8,128]{3,2,1,0:T(8,128)(2,1)}, u32[]{:S(2)}) copy-start(bf16[128,2,8,128]{3,2,1,0:T(8,128)(2,1)} %copy-done.1) | copy-start | bytes 1572868
  335.0 13.6 %copy-start.17 = (f32[2]{0:T(128)S(1)}, f32[2]{0:T(128)}, u32[]{:S(2)}) copy-start(f32[2]{0:T(128)} %copy-done.16) | copy-start | bytes 28
  (4 other events, 6.7 us)
Sparse Core Ops, SparseCore 0:
  9.0 51.1 all-gather.8
  231.8 47.1 all-gather.10
where the time goes:
time: 390 us; the launch traced here: 384 us
  matrix products  134 us (34%)
  blocking collectives  86.9 us (22%)
  local copies, waits for them, and re-layouts  71.2 us (18%)
  waiting for transfers between devices  44.1 us (11%)
  other arithmetic  26.8 us (7%)
  between operations  14 us (4%)
  starting transfers between devices  5.59 us (1%)
    all_gather x3, blocking collectives, per_device(): gathered = lax.all_gather(stacked, 'sp', axis=0, tiled=True)  71.4 us
    all_gather x1, waiting for transfers between devices, per_device(): whole_rows = lax.all_gather(tokens, 'tp', axis=1, tiled=True)  43.3 us
    dot_general x16, matrix products, block_step(): jnp.einsum('hts,hsv->htv', scores, v_blk)  21.4 us
    dot_general x16, matrix products, block_step(): jnp.einsum('hsv,hsk->hvk', v_blk * weights[:, :, None], k_blk)  18.7 us
    dot_general x16, matrix products, block_step(): jnp.einsum('htd,hsd->hts', q_blk, k_blk)  16.9 us
    dot_general x16, matrix products, block_step(): jnp.einsum('hvk,htk->htv', memory, q_blk)  16.6 us
    dot_general x16, matrix products, block_step(): jnp.einsum('hk,htk->ht', normer, q_blk)  15.5 us
    all_to_all x1, blocking collectives, per_device(): owned = lax.all_to_all(mixed, 'tp', split_axis=0, concat_axis=1, tiled=True)  15.5 us
  transfers between devices with their start and end apart: 4, of which 1 were waited for; matrix products, arithmetic and copies ran while one was open for 8% of the time, Pallas kernels for 0%

commit v1 on v0

--- a/solution.py
+++ b/solution.py
@@ -181,7 +181,7 @@
     gate_in = lax.dynamic_slice_in_dim(input_gate_matrix, group_index * head_local, head_local, 2)
     gate_fg = lax.dynamic_slice_in_dim(forget_gate_matrix, group_index * head_local, head_local, 2)
     gate_weight = jnp.concatenate([gate_in, gate_fg], axis=1).reshape(model_width, 4 * head_local)
-    whole_rows = lax.all_gather(tokens, "tp", axis=1, tiled=True)
+    whole_rows = jnp.concatenate(lax.all_gather(tokens, "tp"), axis=1)
     floats = whole_rows.astype(jnp.float32)
     mean_row = jnp.sum(floats, axis=1) / model_width
     variance = jnp.sum(floats * floats, axis=1) / model_width - mean_row * mean_row

time: 390 us -> 416 us (1.067)
  local copies, waits for them, and re-layouts: 71.2 us -> 86.8 us
  other arithmetic: 26.8 us -> 36.5 us
    convert_element_type x0 -> x2, local copies, waits for them, and re-layouts: none -> 15.1 us  [the longest x1 8.75 us: per_device(): floats = whole_rows.astype(jnp.float32)]
    convert_element_type x0 -> x3, other arithmetic: none -> 12 us  [the longest x2 8.67 us: per_device(): normed = ((floats - mean_row[:, None]) * lax.rsqrt(variance + LN_EPS)[:,...]
    unnamed x57 -> x55, local copies, waits for them, and re-layouts: 7.71 us -> 12.9 us
    rev x1, local copies, waits for them, and re-layouts: 5.08 us -> 0.54 us  [per_device(): flipped_query = query_heads[:, ::-1]]
  transfers between devices with their start and end apart: 4 -> 4, of which waited for: 1 -> 1; matrix products, arithmetic and copies ran while one was open for 8% -> 7% of each run, Pallas kernels for 0% -> 0%
where the time goes in v1:
time: 416 us; the launch traced here: 410 us
  matrix products  134 us (32%)
  blocking collectives  88.1 us (21%)
  local copies, waits for them, and re-layouts  86.8 us (21%)
  waiting for transfers between devices  43.4 us (10%)
  other arithmetic  36.5 us (9%)
  between operations  14 us (3%)
  starting transfers between devices  5.97 us (1%)
    all_gather x3, blocking collectives, per_device(): gathered = lax.all_gather(stacked, 'sp', axis=0, tiled=True)  72.5 us
    all_gather x1, waiting for transfers between devices, per_device(): whole_rows = jnp.concatenate(lax.all_gather(tokens, 'tp'), axis=1)  42.6 us
    dot_general x16, matrix products, block_step(): jnp.einsum('hts,hsv->htv', scores, v_blk)  21.3 us
    dot_general x16, matrix products, block_step(): jnp.einsum('hsv,hsk->hvk', v_blk * weights[:, :, None], k_blk)  18.6 us
    dot_general x16, matrix products, block_step(): jnp.einsum('htd,hsd->hts', q_blk, k_blk)  16.9 us
    dot_general x16, matrix products, block_step(): jnp.einsum('hvk,htk->htv', memory, q_blk)  16.6 us
    all_to_all x1, blocking collectives, per_device(): owned = lax.all_to_all(mixed, 'tp', split_axis=0, concat_axis=1, tiled=True)  15.5 us
    dot_general x16, matrix products, block_step(): jnp.einsum('hk,htk->ht', normer, q_blk)  15.5 us
  transfers between devices with their start and end apart: 4, of which 1 were waited for; matrix products, arithmetic and copies ran while one was open for 7% of the time, Pallas kernels for 0%

profile of v1, /device:TPU:1, one launch (start us, length us, event | category | flops | bytes accessed | tf_op | source)
XLA Modules:
  0.0 409.6 jit_solution(14835070516339681995)
XLA Ops:
  17.6 42.6 %all-gather.10.cloned.1.call-done = bf16[4096,512]{1,0:T(8,128)(2,1)} async-done(((bf16[1024,512]{1,0:T(8,128)(2,1)}), bf16[4096,512]{1,0:T(8,128)(2,1)}) %all-gather.10.cloned.1.call-update) | async-done | bytes 4194320 | tf_op jit(solution)/shard_map/all_gather | solution.py:184
  60.2 3.4 convert_element_type.145
  64.3 3.6 copy-done.1
  69.5 8.8 %copy.202 = f32[1024,4,512]{0,2,1:T(8,128)} copy(f32[1024,4,512]{2,0,1:T(8,128)} %bitcast.511) | data formatting | bytes 16777216 | tf_op jit(solution)/shard_map/convert_element_type | solution.py:185
  78.3 5.4 %fusion.68 = bf16[1024,2048]{0,1:T(8,128)(2,1)} fusion(f32[1024,4,512]{0,2,1:T(8,128)} %copy.202, f32[2048]{0:T(1024)S(1)} %copy-done.15, f32[1024]{0:T(1024)S(1)} %get-tuple-element.468, f32[1024]{0:T(1024)S(1)} %get-tuple-element.467), kind=kLoop, calls=%fused_computation.113 | loop fusion | flops 8388608 | bytes 12599296 | tf_op jit(solution)/shard_map/convert_element_type | solution.py:190
  84.4 3.3 fusion.69
  87.7 6.3 %copy.204 = bf16[1024,4,512]{0,2,1:T(8,128)(2,1)} copy(bf16[1024,4,512]{2,0,1:T(8,128)(2,1)} %fusion.69) | data formatting | bytes 8388608 | tf_op jit(solution)/shard_map/convert_element_type | solution.py:190
  94.0 3.0 fusion.173
  98.6 8.9 %convolution_convert_fusion = bf16[1024,1152]{1,0:T(8,128)(2,1)S(1)} fusion(bf16[1024,2048]{0,1:T(8,128)(2,1)} %fusion.68, bf16[2048,1152]{1,0:T(8,128)(2,1)} %constant_dynamic-update-slice_fusion.4), kind=kOutput, calls=%fused_computation.123 | convolution fusion | flops 4833017856 | bytes 11272192 | tf_op jit(solution)/shard_map/dot_general | solution.py:191
  112.5 8.2 %rev.21 = bf16[2,1024,128]{2,1,0:T(8,128)(2,1)} reverse(bf16[2,1024,128]{2,1,0:T(8,128)(2,1)} %get-tuple-element.451), dimensions={1} | reverse | bytes 1048576 | tf_op jit(solution)/shard_map/rev | solution.py:224
  122.1 5.1 %rev.20 = f32[2,1024,128]{2,1,0:T(8,128)} reverse(f32[2,1024,128]{2,1,0:T(8,128)S(1)} %bitcast.514), dimensions={1} | reverse | bytes 2097152 | tf_op jit(solution)/shard_map/rev | solution.py:225
  128.2 66.1 %while.43 = (s32[]{:T(128)}, f32[2,128,128]{2,1,0:T(8,128)S(1)}, f32[2,128]{1,0:T(2,128)S(1)}, f32[2]{0:T(128)S(1)}, f32[8,2,128,128]{3,2,1,0:T(8,128)}, /*index...) while((s32[]{:T(128)}, f32[2,128,128]{2,1,0:T(8,128)S(1)}, ...), condition=%wide.region_18.19_spmd.clone, body=%wide.region_13.18_spmd.clone.sunk | while | flops 34327816 | bytes 1601322 | solution.py:75
  197.4 58.2 %while.42 = (s32[]{:T(128)}, f32[2,128,128]{2,1,0:T(8,128)S(1)}, f32[2,128]{1,0:T(2,128)S(1)}, f32[2]{0:T(128)S(1)}, f32[8,2,128,128]{3,2,1,0:T(8,128)}, /*index...) while((s32[]{:T(128)}, f32[2,128,128]{2,1,0:T(8,128)S(1)}, ...), condition=%wide.region_7.8_spmd.clone, body=%wide.region_2.7_spmd.clone.sunk | while | flops 34327816 | bytes 1601826 | solution.py:75
  259.1 3.8 collective-permute-start
  267.5 26.9 %all-gather.5 = f32[32,2,2]{2,1,0:T(2,128)S(1)} all-gather(f32[1,2,2]{2,1,0:T(2,128)S(1)} %maximum_bitcast_fusion), channel_id=3, replica_groups=mesh['sp'=32,'tp'=4] {'sp'}, dimensions={0}, use_global_device_ids=true | all-gather | bytes 528 | tf_op jit(solution)/shard_map/all_gather | solution.py:255
  294.8 21.8 %all-gather.6 = f32[32,2,2]{2,1,0:T(2,128)S(1)} all-gather(f32[1,2,2]{2,1,0:T(2,128)S(1)} %maximum_bitcast_fusion.1), channel_id=4, replica_groups=mesh['sp'=32,'tp'=4] {'sp'}, dimensions={0}, use_global_device_ids=true | all-gather | bytes 528 | tf_op jit(solution)/shard_map/all_gather | solution.py:255
  317.3 23.8 %all-gather.4 = bf16[64,2,128]{2,1,0:T(2,128)(2,1)S(1)} all-gather(bf16[2,2,128]{2,1,0:T(2,128)(2,1)S(1)} %pad_maximum_fusion.3), channel_id=6, replica_groups=mesh['sp'=32,'tp'=4] {'sp'}, dimensions={0}, use_global_device_ids=true | all-gather | bytes 33792 | tf_op jit(solution)/shard_map/all_gather | solution.py:255
  344.4 2.6 copy.232
  350.8 2.4 reshape.665
  355.4 4.2 %slice_bitcast_fusion.1 = (bf16[32,2,128,128]{3,2,1,0:T(8,128)(2,1)}, bf16[32,2,128,128]{3,2,1,0:T(8,128)(2,1)S(1)}) fusion(bf16[32,2,2,128,128]{4,3,2,1,0:T(8,128)(2,1)} %bitcast.518), kind=kLoop, calls=%fused_computation.118 | loop fusion | bytes 8388608 | tf_op jit(solution)/shard_map/squeeze | solution.py:256
  362.3 9.4 %rev.23 = f32[2,1024,128]{1,2,0:T(8,128)} reverse(f32[2,1024,128]{1,2,0:T(8,128)} %fusion.79), dimensions={1} | reverse | bytes 2097152 | tf_op jit(solution)/shard_map/rev | solution.py:269
  371.7 2.8 fusion.72
  381.9 15.5 %all_to_all.16 = bf16[4,256,384]{1,2,0:T(8,128)(2,1)S(1)} all-to-all(bf16[4,256,384]{1,2,0:T(8,128)(2,1)} %copy.235), channel_id=1, replica_groups=mesh['sp'=32,'tp'=4] {'tp'}, dimensions={0} | all-to-all | bytes 1572864 | tf_op jit(solution)/shard_map/all_to_all | solution.py:281
  397.5 3.5 fusion.175
  (453 shorter events, 179.0 us)
Async XLA Ops:
  6.5 394.5 %copy-start = (bf16[512,2048]{1,0:T(8,128)(2,1)S(1)}, bf16[512,2048]{1,0:T(8,128)(2,1)}, u32[]{:S(2)}) copy-start(bf16[512,2048]{1,0:T(8,128)(2,1)} %param.42) | copy-start | bytes 6291460
  6.5 7.8 %copy-start.11 = (bf16[2048,256]{1,0:T(8,128)(2,1)S(1)}, bf16[2048,256]{1,0:T(8,128)(2,1)}, u32[]{:S(2)}) copy-start(bf16[2048,256]{1,0:T(8,128)(2,1)} %param.28) | copy-start | bytes 3145732
  6.5 53.7 %all-gather.10.cloned.1.call-start = ((), (), s32[]{:S(2)}) async-start(), calls=%async_computation.1 | async-start | bytes 5242880 | tf_op jit(solution)/shard_map/all_gather | solution.py:184
  7.3 348.1 %all-gather.12.cloned.1.call-start = ((), (), s32[]{:S(2)}) async-start(), calls=%async_computation.2 | async-start | bytes 4325376 | tf_op jit(solution)/shard_map/all_gather | solution.py:255
  9.1 6.3 %copy-start.12 = (bf16[2048,256]{1,0:T(8,128)(2,1)S(1)}, bf16[2048,256]{1,0:T(8,128)(2,1)}, u32[]{:S(2)}) copy-start(bf16[2048,256]{1,0:T(8,128)(2,1)} %param.29) | copy-start | bytes 3145732
  9.2 7.4 %copy-start.13 = (bf16[2048,256]{1,0:T(8,128)(2,1)S(1)}, bf16[2048,256]{1,0:T(8,128)(2,1)}, u32[]{:S(2)}) copy-start(bf16[2048,256]{1,0:T(8,128)(2,1)} %param.30) | copy-start | bytes 3145732
  63.6 4.3 %copy-start.1 = (f32[4096,512]{1,0:T(8,128)}, f32[4096,512]{1,0:T(8,128)S(1)}, u32[]{:S(2)}) copy-start(f32[4096,512]{1,0:T(8,128)S(1)} %convert_element_type.145) | copy-start | bytes 25165828
  63.6 5.2 %copy-start.2 = (bf16[4096,512]{1,0:T(8,128)(2,1)S(1)}, bf16[4096,512]{1,0:T(8,128)(2,1)}, u32[]{:S(2)}) copy-start(bf16[4096,512]{1,0:T(8,128)(2,1)} %all-gather.10.cloned.1.call-done) | copy-start | bytes 12582916
  69.5 8.8 %copy-start.15 = (f32[2048]{0:T(1024)S(1)}, f32[2048]{0:T(1024)}, u32[]{:S(2)}) copy-start(f32[2048]{0:T(1024)} %param.25) | copy-start | bytes 24580
  78.3 6.2 %copy-start.3 = (bf16[4096,512]{1,0:T(8,128)(2,1)S(1)}, bf16[4096,512]{1,0:T(8,128)(2,1)}, u32[]{:S(2)}) copy-start(bf16[4096,512]{1,0:T(8,128)(2,1)} %all-gather.10.cloned.1.call-done) | copy-start | bytes 12582916
  107.5 3.5 copy-start.10
  111.0 9.7 %copy-start.6 = (bf16[2,1024,128]{2,1,0:T(8,128)(2,1)}, bf16[2,1024,128]{2,1,0:T(8,128)(2,1)S(1)}, u32[]{:S(2)}) copy-start(bf16[2,1024,128]{2,1,0:T(8,128)(2,1)S(1)} %get-tuple-element.477) | copy-start | bytes 1572868
  111.6 9.2 %copy-start.7 = (bf16[2,1024,128]{2,1,0:T(8,128)(2,1)}, bf16[2,1024,128]{2,1,0:T(8,128)(2,1)S(1)}, u32[]{:S(2)}) copy-start(bf16[2,1024,128]{2,1,0:T(8,128)(2,1)S(1)} %rev.22) | copy-start | bytes 1572868
  197.4 119.4 %copy-start.19 = (f32[2,2]{1,0:T(2,128)S(1)}, f32[2,2]{1,0:T(2,128)}, u32[]{:S(2)}) copy-start(f32[2,2]{1,0:T(2,128)} %param.38) | copy-start | bytes 52
  197.4 144.0 %copy-start.18 = (f32[2,2,128]{2,1,0:T(2,128)S(1)}, f32[2,2,128]{2,1,0:T(2,128)}, u32[]{:S(2)}) copy-start(f32[2,2,128]{2,1,0:T(2,128)} %param.37) | copy-start | bytes 6148
  255.6 93.8 %copy-start.9 = (f32[8,2,128,128]{3,2,1,0:T(8,128)S(1)}, f32[8,2,128,128]{3,2,1,0:T(8,128)}, u32[]{:S(2)}) copy-start(f32[8,2,128,128]{3,2,1,0:T(8,128)} %get-tuple-element.142) | copy-start | bytes 3145732
  259.1 94.1 %collective-permute-start = (bf16[8,128]{1,0:T(8,128)(2,1)S(1)}, bf16[8,128]{1,0:T(8,128)(2,1)S(1)}, u32[]{:S(2)}, u32[]{:S(2)}) collective-permute-start(bf16[8,128]{1,0:T(8,128)(2,1)S(1)} %get-tuple-element.443), channel_id=1, source_target_pairs={{0,4},{4,8},{8,12},{12,16},{16,20},{20,24},{24,28},{28,32},{32,36}... | collective-permute-start | bytes 6152 | tf_op jit(solution)/shard_map/ppermute | solution.py:19
  263.0 90.2 %collective-permute-start.1 = (bf16[8,128]{1,0:T(8,128)(2,1)S(1)}, bf16[8,128]{1,0:T(8,128)(2,1)S(1)}, u32[]{:S(2)}, u32[]{:S(2)}) collective-permute-start(bf16[8,128]{1,0:T(8,128)(2,1)S(1)} %get-tuple-element.444), channel_id=1, source_target_pairs={{4,0},{8,4},{12,8},{16,12},{20,16},{24,20},{28,24},{32,28},{36,32}... | collective-permute-start | bytes 6152 | tf_op jit(solution)/shard_map/ppermute | solution.py:22
  344.4 8.8 %slice-start = ((bf16[1024,1152]{1,0:T(8,128)(2,1)}), bf16[1024,128]{1,0:T(8,128)(2,1)S(1)}, s32[]{:S(2)}) async-start(bf16[1024,1152]{1,0:T(8,128)(2,1)} %copy-done.10), calls=%async_computation.3 | async-start | bytes 524288 | tf_op jit(solution)/shard_map/slice | solution.py:193
  344.4 8.8 %copy-start.21 = (f32[128]{0:T(128)S(1)}, f32[128]{0:T(128)}, u32[]{:S(2)}) copy-start(f32[128]{0:T(128)} %dynamic_slice.60) | copy-start | bytes 1540
  355.4 5.5 %copy-start.8 = (bf16[2,1024,128]{2,1,0:T(8,128)(2,1)S(1)}, bf16[2,1024,128]{2,1,0:T(8,128)(2,1)}, u32[]{:S(2)}) copy-start(bf16[2,1024,128]{2,1,0:T(8,128)(2,1)} %copy-done.7) | copy-start | bytes 1572868
  355.4 5.5 %copy-start.14 = (f32[2,1024,128]{1,2,0:T(8,128)S(1)}, f32[2,1024,128]{1,2,0:T(8,128)}, u32[]{:S(2)}) copy-start(f32[2,1024,128]{1,2,0:T(8,128)} %reshape.668) | copy-start | bytes 3145732
  355.4 5.5 %copy-start.20 = (f32[2,2,128,128]{3,2,1,0:T(8,128)S(1)}, f32[2,2,128,128]{3,2,1,0:T(8,128)}, u32[]{:S(2)}) copy-start(f32[2,2,128,128]{3,2,1,0:T(8,128)} %param.36) | copy-start | bytes 786436
  360.9 13.6 %copy-start.5 = (bf16[128,2,8,128]{3,2,1,0:T(8,128)(2,1)S(1)}, bf16[128,2,8,128]{3,2,1,0:T(8,128)(2,1)}, u32[]{:S(2)}) copy-start(bf16[128,2,8,128]{3,2,1,0:T(8,128)(2,1)} %copy-done.4) | copy-start | bytes 1572868
  (3 other events, 6.9 us)
Sparse Core Ops, SparseCore 0:
  9.0 51.1 all-gather.9
  256.4 47.1 all-gather.11
